TPU v7x, 32 devices: a whole 2x2x4 slice. The times are simulated.
32 devices in a mesh: grp: 2 (over y), fs: 4 (over z), tp: 4 (over x, core).
Axes of the slice: x: 2, y: 2, z: 4, core: 2. Of those that a mesh axis runs over, the one named last changes fastest.
Arguments:
- tokens: bfloat16 [4096, 2048], P(('grp', 'fs')), parts along dimension 0, may hold values from -6 to 6
- norm_gain: float32 [2, 2048], replicated, may hold values from 0.1 to 1.9
- norm_shift: float32 [2, 2048], replicated, may hold values from -3 to 3
- gate_first: bfloat16 [2048, 3072], P('fs', 'tp'), may hold values from -0.125 to 0.125
- up_first: bfloat16 [2048, 3072], P('fs', 'tp'), may hold values from -0.125 to 0.125
- down_first: bfloat16 [3072, 2048], P('tp', 'fs'), may hold values from -0.21875 to 0.21875
- gate_second: bfloat16 [2048, 3072], P('fs', 'tp'), may hold values from -0.125 to 0.125
- up_second: bfloat16 [2048, 3072], P('fs', 'tp'), may hold values from -0.125 to 0.125
- down_second: bfloat16 [3072, 2048], P('tp', 'fs'), may hold values from -0.21875 to 0.21875
Outputs:
- encoded: bfloat16 [4096, 2048], P(('grp', 'fs')), parts along dimension 0
There are 2 independent parts, one for each index of `grp`. A program takes and returns all parts, laid end to end along the dimension named above; an argument that names none is the same for every part. Nothing has to cross between parts.
All inputs are finite; a program needn't handle non-finite values.
Results may differ from a plain program's by a relative error of at most 0.012.
Values may be sent and summed in bfloat16 or wider, within the bound.
A program may use at most 64 MiB of HBM per device.

v0:
```python
import jax
import jax.numpy as jnp
from jax import lax
from jax.sharding import PartitionSpec as P


def post_norm(values, gain, shift):
    mean = jnp.mean(values, axis=-1, keepdims=True)
    spread = jnp.mean(jnp.square(values - mean), axis=-1, keepdims=True)
    normed = (values - mean) * lax.rsqrt(spread + 1e-05)
    return (normed * gain + shift).astype(jnp.bfloat16)


def rounded_term(stream_rows, down_full):
    return jnp.dot(stream_rows, down_full, preferred_element_type=jnp.float32).astype(jnp.bfloat16)


def half_step(stream, gate_w, up_w, down_w, gain, shift):
    width = gate_w.shape[1]
    joined = jnp.concatenate(
        (
            lax.all_gather(gate_w, "fs", axis=0, tiled=True),
            lax.all_gather(up_w, "fs", axis=0, tiled=True),
        ),
        axis=1,
    )
    both = jnp.dot(stream, joined, preferred_element_type=jnp.float32)
    gate = both[:, :width]
    up = both[:, width:]
    hidden = (jax.nn.silu(gate) * up).astype(jnp.bfloat16)
    scale = 2.0**0.25
    down_full = lax.all_gather(down_w, "fs", axis=1, tiled=True)
    partial_value = rounded_term(hidden, down_full)
    branch = lax.psum(partial_value, "tp").astype(jnp.float32).astype(jnp.bfloat16)
    return post_norm(
        scale * stream.astype(jnp.float32) + 0.5 * branch.astype(jnp.float32), gain, shift
    )


def local(
    tokens,
    norm_gain,
    norm_shift,
    gate_first,
    up_first,
    down_first,
    gate_second,
    up_second,
    down_second,
):
    middle = half_step(tokens, gate_first, up_first, down_first, norm_gain[0], norm_shift[0])
    return half_step(middle, gate_second, up_second, down_second, norm_gain[1], norm_shift[1])


def solution(mesh):
    placed = (
        P(("grp", "fs"), None),
        P(),
        P(),
        P("fs", "tp"),
        P("fs", "tp"),
        P("tp", "fs"),
        P("fs", "tp"),
        P("fs", "tp"),
        P("tp", "fs"),
    )
    return jax.shard_map(
        local, mesh=mesh, in_specs=placed, out_specs=P(("grp", "fs"), None), check_vma=False
    )
```

profile of v0, /device:TPU:0, one launch (start us, length us, event | category | flops | bytes accessed | tf_op | source)
XLA Modules:
  0.0 519.6 jit_solution(14808185520538437367)
XLA Ops:
  6.5 0.7 all-gather.7.cloned.1.call-update
  7.3 0.7 all-gather.9.cloned.1.call-update
  8.1 0.7 all-gather.11.cloned.1.call-update
  8.8 66.3 %all-gather.7.cloned.1.call-done = bf16[2048,768]{1,0:T(8,128)(2,1)} async-done(((bf16[512,768]{1,0:T(8,128)(2,1)}), bf16[2048,768]{1,0:T(8,128)(2,1)}) %all-gather.7.cloned.1.call-update) | async-done | bytes 3145744 | tf_op jit(solution)/shard_map/all_gather | solution.py:22
  75.1 63.7 %all-gather.9.cloned.1.call-done = bf16[2048,768]{1,0:T(8,128)(2,1)} async-done(((bf16[512,768]{1,0:T(8,128)(2,1)}), bf16[2048,768]{1,0:T(8,128)(2,1)}) %all-gather.9.cloned.1.call-update) | async-done | bytes 3145744 | tf_op jit(solution)/shard_map/all_gather | solution.py:23
  138.8 6.9 %fusion.8 = f32[512,1536]{0,1:T(8,128)S(1)} fusion(bf16[512,2048]{1,0:T(8,128)(2,1)} %param.9, bf16[2048,768]{1,0:T(8,128)(2,1)} %all-gather.9.cloned.1.call-done, bf16[2048,768]{1,0:T(8,128)(2,1)} %all-gather.7.cloned.1.call-done), kind=kOutput, calls=%fused_computation.14 | convolution fusion | flops 3233808384 | bytes 11534336 | tf_op jit(solution)/shard_map/dot_general | solution.py:27
  145.7 56.7 %all-gather.11.cloned.1.call-done = bf16[768,2048]{1,0:T(8,128)(2,1)} async-done(((bf16[768,512]{1,0:T(8,128)(2,1)}), bf16[768,2048]{1,0:T(8,128)(2,1)}) %all-gather.11.cloned.1.call-update) | async-done | bytes 3145744 | tf_op jit(solution)/shard_map/all_gather | solution.py:32
  202.5 5.1 convolution_convert_fusion.1
  207.7 0.5 all-gather.13.cloned.1.call-update
  208.3 0.5 all-gather.15.cloned.1.call-update
  208.8 0.7 all-gather.17.cloned.1.call-update
  209.8 48.0 %all-reduce.3.cloned.1.call-done = bf16[512,2048]{1,0:T(8,128)(2,1)} async-done(((bf16[512,2048]{1,0:T(8,128)(2,1)}), bf16[512,2048]{1,0:T(8,128)(2,1)}) %all-reduce.3.cloned.1.call-update) | async-done | bytes 2097168 | tf_op jit(solution)/shard_map/psum | solution.py:34
  257.8 2.6 fusion.11
  260.5 1.2 multiply_reduce_fusion.1
  262.0 1.3 add_convert_fusion.1
  263.4 59.4 %all-gather.13.cloned.1.call-done = bf16[2048,768]{1,0:T(8,128)(2,1)} async-done(((bf16[512,768]{1,0:T(8,128)(2,1)}), bf16[2048,768]{1,0:T(8,128)(2,1)}) %all-gather.13.cloned.1.call-update) | async-done | bytes 3145744 | tf_op jit(solution)/shard_map/all_gather | solution.py:22
  322.8 63.5 %all-gather.15.cloned.1.call-done = bf16[2048,768]{1,0:T(8,128)(2,1)} async-done(((bf16[512,768]{1,0:T(8,128)(2,1)}), bf16[2048,768]{1,0:T(8,128)(2,1)}) %all-gather.15.cloned.1.call-update) | async-done | bytes 3145744 | tf_op jit(solution)/shard_map/all_gather | solution.py:23
  386.3 8.0 %fusion.4 = f32[512,1536]{0,1:T(8,128)} fusion(bf16[512,2048]{1,0:T(8,128)(2,1)S(1)} %add_convert_fusion.1, bf16[2048,768]{1,0:T(8,128)(2,1)} %all-gather.15.cloned.1.call-done, bf16[2048,768]{1,0:T(8,128)(2,1)} %all-gather.13.cloned.1.call-done), kind=kOutput, calls=%fused_computation.4 | convolution fusion | flops 3233808384 | bytes 11534336 | tf_op jit(solution)/shard_map/dot_general | solution.py:27
  394.3 55.7 %all-gather.17.cloned.1.call-done = bf16[768,2048]{1,0:T(8,128)(2,1)} async-done(((bf16[768,512]{1,0:T(8,128)(2,1)}), bf16[768,2048]{1,0:T(8,128)(2,1)}) %all-gather.17.cloned.1.call-update) | async-done | bytes 3145744 | tf_op jit(solution)/shard_map/all_gather | solution.py:32
  450.0 6.1 %convolution_convert_fusion = bf16[512,2048]{1,0:T(8,128)(2,1)} fusion(bf16[768,2048]{1,0:T(8,128)(2,1)} %all-gather.17.cloned.1.call-done, f32[512,1536]{0,1:T(8,128)} %fusion.4), kind=kOutput, calls=%fused_computation.15 | convolution fusion | flops 1614020608 | bytes 8388608 | tf_op jit(solution)/shard_map/dot_general | solution.py:15
  456.1 50.2 %all-reduce.5.cloned.1.call-done = bf16[512,2048]{1,0:T(8,128)(2,1)} async-done(((bf16[512,2048]{1,0:T(8,128)(2,1)}), bf16[512,2048]{1,0:T(8,128)(2,1)}) %all-reduce.5.cloned.1.call-update) | async-done | bytes 2097168 | tf_op jit(solution)/shard_map/psum | solution.py:34
  506.3 2.6 fusion.12
  508.9 1.2 multiply_reduce_fusion
  510.1 2.6 add_convert_fusion
  (28 shorter events, 1.0 us)
Async XLA Ops:
  6.5 68.6 %all-gather.7.cloned.1.call-start = ((), (), s32[]{:S(2)}) async-start(), calls=%async_computation | async-start | bytes 3932160 | tf_op jit(solution)/shard_map/all_gather | solution.py:22
  7.3 131.5 %all-gather.9.cloned.1.call-start = ((), (), s32[]{:S(2)}) async-start(), calls=%async_computation.1 | async-start | bytes 3932160 | tf_op jit(solution)/shard_map/all_gather | solution.py:23
  8.0 194.5 %all-gather.11.cloned.1.call-start = ((), (), s32[]{:S(2)}) async-start(), calls=%async_computation.2 | async-start | bytes 3932160 | tf_op jit(solution)/shard_map/all_gather | solution.py:32
  8.7 249.1 %all-reduce.3.cloned.1.call-start = ((), (), s32[]{:S(2)}) async-start(), calls=%async_computation.3 | async-start | bytes 4194304 | tf_op jit(solution)/shard_map/psum | solution.py:34
  207.6 2.2 copy-start.4
  207.6 2.2 copy-start.5
  207.6 50.2 %copy-start = (bf16[512,2048]{1,0:T(8,128)(2,1)S(1)}, bf16[512,2048]{1,0:T(8,128)(2,1)}, u32[]{:S(2)}) copy-start(bf16[512,2048]{1,0:T(8,128)(2,1)} %param.9) | copy-start | bytes 6291460
  207.6 115.1 %all-gather.13.cloned.1.call-start = ((), (), s32[]{:S(2)}) async-start(), calls=%async_computation.4 | async-start | bytes 3932160 | tf_op jit(solution)/shard_map/all_gather | solution.py:22
  208.2 178.1 %all-gather.15.cloned.1.call-start = ((), (), s32[]{:S(2)}) async-start(), calls=%async_computation.5 | async-start | bytes 3932160 | tf_op jit(solution)/shard_map/all_gather | solution.py:23
  208.8 241.2 %all-gather.17.cloned.1.call-start = ((), (), s32[]{:S(2)}) async-start(), calls=%async_computation.6 | async-start | bytes 3932160 | tf_op jit(solution)/shard_map/all_gather | solution.py:32
  209.5 296.7 %all-reduce.5.cloned.1.call-start = ((), (), s32[]{:S(2)}) async-start(), calls=%async_computation.7 | async-start | bytes 4194304 | tf_op jit(solution)/shard_map/psum | solution.py:34
  257.8 2.6 copy-start.2
  260.4 1.6 copy-start.1
  506.3 2.6 copy-start.3
Sparse Core Ops, SparseCore 0:
  8.9 66.1 all-gather.6
  76.7 62.0 all-gather.8
  140.4 62.0 all-gather.10
  207.7 50.0 all-reduce.2
  259.2 63.5 all-gather.12
  324.2 62.0 all-gather.14
  387.9 62.0 all-gather.16
  456.2 49.9 all-reduce.4
where the time goes:
time: 520 us
  waiting for transfers between devices  467 us (90%)
  matrix products  26.1 us (5%)
  between operations  13.6 us (3%)
  other arithmetic  11.6 us (2%)
    all_gather x2, waiting for transfers between devices, half_step(): lax.all_gather(up_w, 'fs', axis=0, tiled=True)  127 us
    all_gather x2, waiting for transfers between devices, half_step(): lax.all_gather(gate_w, 'fs', axis=0, tiled=True)  126 us
    all_gather x2, waiting for transfers between devices, half_step(): down_full = lax.all_gather(down_w, 'fs', axis=1, tiled=True)  112 us
    psum x2, waiting for transfers between devices, half_step(): lax.psum(partial_value, 'tp').astype(jnp.float32).astype(jnp.bfloat16)  98.1 us
    dot_general x2, matrix products, half_step(): both = jnp.dot(stream, joined, preferred_element_type=jnp.float32)  14.9 us
    dot_general x2, matrix products, rounded_term(): jnp.dot(stream_rows, down_full, preferred_element_type=jnp.float32)  11.2 us
  transfers between devices with their start and end apart: 8, of which 8 were waited for; matrix products, arithmetic and copies ran while one was open for 4% of the time, Pallas kernels for 0%

commit v1 on v0

--- a/solution.py
+++ b/solution.py
@@ -29,7 +29,12 @@
     up = both[:, width:]
     hidden = (jax.nn.silu(gate) * up).astype(jnp.bfloat16)
     scale = 2.0**0.25
-    down_full = lax.all_gather(down_w, "fs", axis=1, tiled=True)
+    ring = [down_w]
+    for hop in range(3):
+        ring.append(lax.ppermute(ring[-1], "fs", [(dev, (dev + 1) % 4) for dev in range(4)]))
+    down_full = jnp.roll(
+        jnp.concatenate(ring[::-1], axis=1), (lax.axis_index("fs") + 1) * ring[0].shape[1], axis=1
+    )
     partial_value = rounded_term(hidden, down_full)
     branch = lax.psum(partial_value, "tp").astype(jnp.float32).astype(jnp.bfloat16)
     return post_norm(

time: 520 us -> 439 us (0.84)
  waiting for transfers between devices: 467 us -> 357 us
  starting transfers between devices: 0.45 us -> 26 us
    all_gather x2 -> x0, waiting for transfers between devices: 112 us -> none  [half_step(): down_full = lax.all_gather(down_w, 'fs', axis=1, tiled=True)]
    ppermute x0 -> x6, waiting for transfers between devices: none -> 105 us  [half_step(): lax.ppermute(ring[-1], 'fs', [(dev, (dev + 1) % 4) for dev in range(4)])]
    all_gather x2, waiting for transfers between devices: 126 us -> 64.7 us  [half_step(): lax.all_gather(gate_w, 'fs', axis=0, tiled=True)]
    psum x2, waiting for transfers between devices: 98.1 us -> 57.7 us  [half_step(): lax.psum(partial_value, 'tp').astype(jnp.float32).astype(jnp.bfloat16)]
    ppermute x0 -> x6, starting transfers between devices: none -> 25.8 us  [half_step(): lax.ppermute(ring[-1], 'fs', [(dev, (dev + 1) % 4) for dev in range(4)])]
  transfers between devices with their start and end apart: 8 -> 12, of which waited for: 8 -> 10; matrix products, arithmetic and copies ran while one was open for 4% -> 4% of each run, Pallas kernels for 0% -> 0%
where the time goes in v1:
time: 439 us
  waiting for transfers between devices  357 us (81%)
  matrix products  29.1 us (7%)
  starting transfers between devices  26 us (6%)
  between operations  13.6 us (3%)
  other arithmetic  11.6 us (3%)
    all_gather x2, waiting for transfers between devices, half_step(): lax.all_gather(up_w, 'fs', axis=0, tiled=True)  128 us
    ppermute x6, waiting for transfers between devices, half_step(): lax.ppermute(ring[-1], 'fs', [(dev, (dev + 1) % 4) for dev in range(4)])  105 us
    all_gather x2, waiting for transfers between devices, half_step(): lax.all_gather(gate_w, 'fs', axis=0, tiled=True)  64.7 us
    psum x2, waiting for transfers between devices, half_step(): lax.psum(partial_value, 'tp').astype(jnp.float32).astype(jnp.bfloat16)  57.7 us
    ppermute x6, starting transfers between devices, half_step(): lax.ppermute(ring[-1], 'fs', [(dev, (dev + 1) % 4) for dev in range(4)])  25.8 us
    dot_general x2, matrix products, rounded_term(): jnp.dot(stream_rows, down_full, preferred_element_type=jnp.float32)  15.7 us
    dot_general x2, matrix products, half_step(): both = jnp.dot(stream, joined, preferred_element_type=jnp.float32)  13.3 us
  transfers between devices with their start and end apart: 12, of which 10 were waited for; matrix products, arithmetic and copies ran while one was open for 4% of the time, Pallas kernels for 0%

profile of v1, /device:TPU:0, one launch (start us, length us, event | category | flops | bytes accessed | tf_op | source)
XLA Modules:
  0.0 439.0 jit_solution(11697023010182053014)
XLA Ops:
  8.1 3.1 collective-permute-start
  11.2 27.4 %collective-permute-done = bf16[768,512]{1,0:T(8,128)(2,1)S(1)} collective-permute-done((bf16[768,512]{1,0:T(8,128)(2,1)}, bf16[768,512]{1,0:T(8,128)(2,1)S(1)}, u32[]{:S(2)}, u32[]{:S(2)}) %collective-permute-start) | collective-permute-done | bytes 786464 | tf_op jit(solution)/shard_map/ppermute | solution.py:34
  38.6 9.3 %collective-permute-start.1 = (bf16[768,512]{1,0:T(8,128)(2,1)S(1)}, bf16[768,512]{1,0:T(8,128)(2,1)S(1)}, u32[]{:S(2)}, u32[]{:S(2)}) collective-permute-start(bf16[768,512]{1,0:T(8,128)(2,1)S(1)} %collective-permute-done), channel_id=1, source_target_pairs={{0,4},{4,8},{8,12},{12,0},{1,5},{5,9},{9,13},{13,1},{2,6},{6,10},{... | collective-permute-start | bytes 2359304 | tf_op jit(solution)/shard_map/ppermute | solution.py:34
  47.9 36.5 %collective-permute-done.1 = bf16[768,512]{1,0:T(8,128)(2,1)S(1)} collective-permute-done((bf16[768,512]{1,0:T(8,128)(2,1)S(1)}, bf16[768,512]{1,0:T(8,128)(2,1)S(1)}, u32[]{:S(2)}, u32[]{:S(2)}) %collective-permute-start.1) | collective-permute-done | bytes 786464 | tf_op jit(solution)/shard_map/ppermute | solution.py:34
  84.4 13.3 %collective-permute-start.2 = (bf16[768,512]{1,0:T(8,128)(2,1)S(1)}, bf16[768,512]{1,0:T(8,128)(2,1)S(1)}, u32[]{:S(2)}, u32[]{:S(2)}) collective-permute-start(bf16[768,512]{1,0:T(8,128)(2,1)S(1)} %collective-permute-done.1), channel_id=1, source_target_pairs={{0,4},{4,8},{8,12},{12,0},{1,5},{5,9},{9,13},{13,1},{2,6},{6,10},{... | collective-permute-start | bytes 2359304 | tf_op jit(solution)/shard_map/ppermute | solution.py:34
  97.8 1.2 all-gather.5.cloned.1.call-done
  98.9 68.4 %all-gather.7.cloned.1.call-done = bf16[2048,768]{1,0:T(8,128)(2,1)} async-done(((bf16[512,768]{1,0:T(8,128)(2,1)}), bf16[2048,768]{1,0:T(8,128)(2,1)}) %all-gather.7.cloned.1.call-update) | async-done | bytes 3145744 | tf_op jit(solution)/shard_map/all_gather | solution.py:23
  167.3 6.9 %fusion.8 = f32[512,1536]{0,1:T(8,128)S(1)} fusion(bf16[512,2048]{1,0:T(8,128)(2,1)} %param.11, bf16[2048,768]{1,0:T(8,128)(2,1)} %all-gather.7.cloned.1.call-done, bf16[2048,768]{1,0:T(8,128)(2,1)} %all-gather.5.cloned.1.call-done), kind=kOutput, calls=%fused_computation.30 | convolution fusion | flops 3233808384 | bytes 11534336 | tf_op jit(solution)/shard_map/dot_general | solution.py:27
  174.2 7.1 %fusion.31 = bf16[512,2048]{1,0:T(8,128)(2,1)} fusion(s32[]{:T(128)S(6)} %select_n.13, bf16[768,512]{1,0:T(8,128)(2,1)S(1)} %collective-permute-done.2, bf16[768,512]{1,0:T(8,128)(2,1)S(1)} %collective-permute-done.1, bf16[768,512]{1,0:T(8,128)(2,1)S(1)} %collective-permute-done, bf16[768,512]{1,0:T(8,128)(2,1)S(1)} %copy-done.6, f32[512,1536]{0,1:T(8,128)S(1)} %fusion.8), kind=kOutput, calls=%fused_computation.47 | convolution fusion | flops 1639186432 | bytes 8388612 | tf_op jit(solution)/shard_map/dot_general | solution.py:15
  182.6 21.2 %collective-permute-done.3 = bf16[768,512]{1,0:T(8,128)(2,1)S(1)} collective-permute-done((bf16[768,512]{1,0:T(8,128)(2,1)S(1)}, bf16[768,512]{1,0:T(8,128)(2,1)S(1)}, u32[]{:S(2)}, u32[]{:S(2)}) %collective-permute-start.3) | collective-permute-done | bytes 786464 | tf_op jit(solution)/shard_map/ppermute | solution.py:34
  203.9 0.8 copy-done.8
  204.8 19.6 %collective-permute-done.4 = bf16[768,512]{1,0:T(8,128)(2,1)} collective-permute-done((bf16[768,512]{1,0:T(8,128)(2,1)S(1)}, bf16[768,512]{1,0:T(8,128)(2,1)}, u32[]{:S(2)}, u32[]{:S(2)}) %collective-permute-start.4) | collective-permute-done | bytes 786464 | tf_op jit(solution)/shard_map/ppermute | solution.py:34
  224.4 7.6 %all-reduce.3.cloned.1.call-done = bf16[512,2048]{1,0:T(8,128)(2,1)} async-done(((bf16[512,2048]{1,0:T(8,128)(2,1)}), bf16[512,2048]{1,0:T(8,128)(2,1)}) %all-reduce.3.cloned.1.call-update) | async-done | bytes 2097168 | tf_op jit(solution)/shard_map/psum | solution.py:39
  231.9 2.6 fusion.37
  234.6 1.2 multiply_reduce_fusion.1
  236.2 1.3 add_convert_fusion.1
  237.5 59.4 %all-gather.11.cloned.1.call-done = bf16[2048,768]{1,0:T(8,128)(2,1)} async-done(((bf16[512,768]{1,0:T(8,128)(2,1)}), bf16[2048,768]{1,0:T(8,128)(2,1)}) %all-gather.11.cloned.1.call-update) | async-done | bytes 3145744 | tf_op jit(solution)/shard_map/all_gather | solution.py:23
  296.9 63.5 %all-gather.9.cloned.1.call-done = bf16[2048,768]{1,0:T(8,128)(2,1)} async-done(((bf16[512,768]{1,0:T(8,128)(2,1)}), bf16[2048,768]{1,0:T(8,128)(2,1)}) %all-gather.9.cloned.1.call-update) | async-done | bytes 3145744 | tf_op jit(solution)/shard_map/all_gather | solution.py:22
  360.5 6.4 %fusion.4 = f32[512,1536]{0,1:T(8,128)S(1)} fusion(bf16[512,2048]{1,0:T(8,128)(2,1)S(1)} %add_convert_fusion.1, bf16[2048,768]{1,0:T(8,128)(2,1)} %all-gather.11.cloned.1.call-done, bf16[2048,768]{1,0:T(8,128)(2,1)} %all-gather.9.cloned.1.call-done), kind=kOutput, calls=%fused_computation.12 | convolution fusion | flops 3233808384 | bytes 11534336 | tf_op jit(solution)/shard_map/dot_general | solution.py:27
  366.9 8.6 %fusion.34 = bf16[512,2048]{1,0:T(8,128)(2,1)} fusion(s32[]{:T(128)S(6)} %select_n.13, bf16[768,512]{1,0:T(8,128)(2,1)} %collective-permute-done.5, bf16[768,512]{1,0:T(8,128)(2,1)} %collective-permute-done.4, bf16[768,512]{1,0:T(8,128)(2,1)S(1)} %copy-done.9, bf16[768,512]{1,0:T(8,128)(2,1)S(1)} %copy-done.7, f32[512,1536]{0,1:T(8,128)S(1)} %fusion.4), kind=kOutput, calls=%fused_computation.48 | convolution fusion | flops 1639186432 | bytes 8388612 | tf_op jit(solution)/shard_map/dot_general | solution.py:15
  375.6 50.1 %all-reduce.5.cloned.1.call-done = bf16[512,2048]{1,0:T(8,128)(2,1)} async-done(((bf16[512,2048]{1,0:T(8,128)(2,1)}), bf16[512,2048]{1,0:T(8,128)(2,1)}) %all-reduce.5.cloned.1.call-update) | async-done | bytes 2097168 | tf_op jit(solution)/shard_map/psum | solution.py:39
  425.7 2.6 fusion.38
  428.4 1.2 multiply_reduce_fusion
  429.5 2.7 add_convert_fusion
  (42 shorter events, 3.2 us)
Async XLA Ops:
  6.5 92.4 %all-gather.5.cloned.1.call-start = ((), (), s32[]{:S(2)}) async-start(), calls=%async_computation | async-start | bytes 3932160 | tf_op jit(solution)/shard_map/all_gather | solution.py:22
  7.3 160.0 %all-gather.7.cloned.1.call-start = ((), (), s32[]{:S(2)}) async-start(), calls=%async_computation.1 | async-start | bytes 3932160 | tf_op jit(solution)/shard_map/all_gather | solution.py:23
  8.0 223.9 %all-reduce.3.cloned.1.call-start = ((), (), s32[]{:S(2)}) async-start(), calls=%async_computation.2 | async-start | bytes 4194304 | tf_op jit(solution)/shard_map/psum | solution.py:39
  8.1 30.5 %collective-permute-start = (bf16[768,512]{1,0:T(8,128)(2,1)}, bf16[768,512]{1,0:T(8,128)(2,1)S(1)}, u32[]{:S(2)}, u32[]{:S(2)}) collective-permute-start(bf16[768,512]{1,0:T(8,128)(2,1)} %param.16), channel_id=1, source_target_pairs={{0,4},{4,8},{8,12},{12,0},{1,5},{5,9},{9,13},{13,1},{2,6},{6,10},{... | collective-permute-start | bytes 2359304 | tf_op jit(solution)/shard_map/ppermute | solution.py:34
  38.6 45.8 %collective-permute-start.1 = (bf16[768,512]{1,0:T(8,128)(2,1)S(1)}, bf16[768,512]{1,0:T(8,128)(2,1)S(1)}, u32[]{:S(2)}, u32[]{:S(2)}) collective-permute-start(bf16[768,512]{1,0:T(8,128)(2,1)S(1)} %collective-permute-done), channel_id=1, source_target_pairs={{0,4},{4,8},{8,12},{12,0},{1,5},{5,9},{9,13},{13,1},{2,6},{6,10},{... | collective-permute-start | bytes 2359304 | tf_op jit(solution)/shard_map/ppermute | solution.py:34
  84.4 89.8 %collective-permute-start.2 = (bf16[768,512]{1,0:T(8,128)(2,1)S(1)}, bf16[768,512]{1,0:T(8,128)(2,1)S(1)}, u32[]{:S(2)}, u32[]{:S(2)}) collective-permute-start(bf16[768,512]{1,0:T(8,128)(2,1)S(1)} %collective-permute-done.1), channel_id=1, source_target_pairs={{0,4},{4,8},{8,12},{12,0},{1,5},{5,9},{9,13},{13,1},{2,6},{6,10},{... | collective-permute-start | bytes 2359304 | tf_op jit(solution)/shard_map/ppermute | solution.py:34
  97.7 76.5 %copy-start.6 = (bf16[768,512]{1,0:T(8,128)(2,1)S(1)}, bf16[768,512]{1,0:T(8,128)(2,1)}, u32[]{:S(2)}) copy-start(bf16[768,512]{1,0:T(8,128)(2,1)} %param.16) | copy-start | bytes 2359300
  181.3 1.3 copy-start.7
  181.3 22.6 %copy-start.4 = (f32[2,2048]{1,0:T(2,128)S(1)}, f32[2,2048]{1,0:T(2,128)}, u32[]{:S(2)}) copy-start(f32[2,2048]{1,0:T(2,128)} %param.12) | copy-start | bytes 49156
  181.3 22.6 %copy-start.5 = (f32[2,2048]{1,0:T(2,128)S(1)}, f32[2,2048]{1,0:T(2,128)}, u32[]{:S(2)}) copy-start(f32[2,2048]{1,0:T(2,128)} %param.13) | copy-start | bytes 49156
  181.3 50.6 %copy-start = (bf16[512,2048]{1,0:T(8,128)(2,1)S(1)}, bf16[512,2048]{1,0:T(8,128)(2,1)}, u32[]{:S(2)}) copy-start(bf16[512,2048]{1,0:T(8,128)(2,1)} %param.11) | copy-start | bytes 6291460
  181.4 115.6 %all-gather.11.cloned.1.call-start = ((), (), s32[]{:S(2)}) async-start(), calls=%async_computation.4 | async-start | bytes 3932160 | tf_op jit(solution)/shard_map/all_gather | solution.py:23
  181.9 178.5 %all-gather.9.cloned.1.call-start = ((), (), s32[]{:S(2)}) async-start(), calls=%async_computation.3 | async-start | bytes 3932160 | tf_op jit(solution)/shard_map/all_gather | solution.py:22
  182.5 243.2 %all-reduce.5.cloned.1.call-start = ((), (), s32[]{:S(2)}) async-start(), calls=%async_computation.5 | async-start | bytes 4194304 | tf_op jit(solution)/shard_map/psum | solution.py:39
  182.6 21.3 %collective-permute-start.3 = (bf16[768,512]{1,0:T(8,128)(2,1)S(1)}, bf16[768,512]{1,0:T(8,128)(2,1)S(1)}, u32[]{:S(2)}, u32[]{:S(2)}) collective-permute-start(bf16[768,512]{1,0:T(8,128)(2,1)S(1)} %copy-done.7), channel_id=1, source_target_pairs={{0,4},{4,8},{8,12},{12,0},{1,5},{5,9},{9,13},{13,1},{2,6},{6,10},{... | collective-permute-start | bytes 2359304 | tf_op jit(solution)/shard_map/ppermute | solution.py:34
  203.9 0.9 copy-start.8
  203.9 20.5 %collective-permute-start.4 = (bf16[768,512]{1,0:T(8,128)(2,1)S(1)}, bf16[768,512]{1,0:T(8,128)(2,1)}, u32[]{:S(2)}, u32[]{:S(2)}) collective-permute-start(bf16[768,512]{1,0:T(8,128)(2,1)S(1)} %collective-permute-done.3), channel_id=1, source_target_pairs={{0,4},{4,8},{8,12},{12,0},{1,5},{5,9},{9,13},{13,1},{2,6},{6,10},{... | collective-permute-start | bytes 2359304 | tf_op jit(solution)/shard_map/ppermute | solution.py:34
  224.4 142.5 %collective-permute-start.5 = (bf16[768,512]{1,0:T(8,128)(2,1)}, bf16[768,512]{1,0:T(8,128)(2,1)}, u32[]{:S(2)}, u32[]{:S(2)}) collective-permute-start(bf16[768,512]{1,0:T(8,128)(2,1)} %collective-permute-done.4), channel_id=1, source_target_pairs={{0,4},{4,8},{8,12},{12,0},{1,5},{5,9},{9,13},{13,1},{2,6},{6,10},{... | collective-permute-start | bytes 2359304 | tf_op jit(solution)/shard_map/ppermute | solution.py:34
  231.9 2.7 copy-start.2
  234.6 1.6 copy-start.1
  360.5 6.4 %copy-start.9 = (bf16[768,512]{1,0:T(8,128)(2,1)S(1)}, bf16[768,512]{1,0:T(8,128)(2,1)}, u32[]{:S(2)}) copy-start(bf16[768,512]{1,0:T(8,128)(2,1)} %copy-done.8) | copy-start | bytes 2359300
  425.7 2.7 copy-start.3
Sparse Core Ops, SparseCore 0:
  8.9 89.9 all-gather.4
  100.5 66.7 all-gather.6
  181.5 50.4 all-reduce.2
  233.4 63.5 all-gather.10
  298.3 62.0 all-gather.8
  375.7 49.9 all-reduce.4
